TPU v7x, 32 devices: a whole 2x2x4 slice. The times are simulated.
32 devices in a mesh: sp: 8 (over z, x), tp: 4 (over y, core).
Axes of the slice: x: 2, y: 2, z: 4, core: 2. Of those that a mesh axis runs over, the one named last changes fastest.
Arguments:
- queries: bfloat16 [8192, 1536], P('sp', 'tp'), may hold values from -200 to 200
- key_heads: bfloat16 [8192, 512], P('sp', 'tp'), may hold values from -6 to 6
- projected_value_heads: bfloat16 [8192, 512], P('sp', 'tp'), may hold values from -5 to 5
- sink_logit_table: float32 [24], P('tp'), may hold values from 0 to 4
- out_weight: bfloat16 [1536, 3072], P('tp'), may hold values from -1.5 to 1.5
- residual: bfloat16 [8192, 3072], P('sp', 'tp'), may hold values from -16 to 16
- norm_gain: bfloat16 [3072], P('tp'), may hold values from 0.099609375 to 1.8984375
- up_weight: bfloat16 [3072, 12288], P('sp', 'tp'), may hold values from -0.109375 to 0.109375
- down_weight: bfloat16 [12288, 3072], P('tp', 'sp'), may hold values from -0.0546875 to 0.0546875
Outputs:
- result: bfloat16 [8192, 3072], P('sp', 'tp')
All inputs are finite; a program needn't handle non-finite values.
Results may differ from a plain program's by a relative error of at most 0.015.
Values may be sent and summed in bfloat16 or wider, within the bound.
No kernel may reach another device: no remote copies, remote signals or barrier semaphores. Data moves between devices by JAX's collectives and lax.ppermute only.
A program may use at most 128 MiB of HBM per device.

v0:
```python
import jax
import jax.numpy as jnp
from jax import lax
from jax.sharding import PartitionSpec as P

D = 3072
HEAD_SIZE = 64
WINDOW_SPAN = 128
epsilon = 1e-06


def shifted(block, axis, distance):
    devices = range(lax.axis_size(axis))
    route = [(i - distance, i) for i in devices if i - distance in devices]
    return lax.ppermute(block, axis, route)


def attend(queries, key_heads, projected_value_heads, sink_logit_table, previous, offset):
    row_count = queries.shape[0]
    kv_cols = key_heads.shape[1]
    kv_local = kv_cols // HEAD_SIZE
    group_count = queries.shape[1] // kv_cols
    block_count = row_count // WINDOW_SPAN
    extended_keys = jnp.concatenate([previous[:, :kv_cols], key_heads], axis=0)
    extended_values = jnp.concatenate([previous[:, kv_cols:], projected_value_heads], axis=0)

    def banded(source_rows):
        shaped = source_rows.reshape(block_count + 1, WINDOW_SPAN, kv_local, HEAD_SIZE)
        return jnp.concatenate([shaped[:-1], shaped[1:]], axis=1)

    key_band = banded(extended_keys)
    value_band = banded(extended_values)
    query_block_list = queries.reshape(block_count, WINDOW_SPAN, kv_local, group_count, HEAD_SIZE)
    scores = jnp.einsum(
        "nqkgd,nskd->nkgqs", query_block_list, key_band, preferred_element_type=jnp.float32
    ) * HEAD_SIZE ** (-0.5)
    within = jnp.arange(WINDOW_SPAN)[:, None]
    column = jnp.arange(2 * WINDOW_SPAN)[None, :]
    distance = WINDOW_SPAN + within - column
    valid = (distance >= 0) & (distance < WINDOW_SPAN)
    key_pos = (
        offset
        + jnp.arange(block_count)[:, None] * WINDOW_SPAN
        + jnp.arange(2 * WINDOW_SPAN)[None, :]
        - WINDOW_SPAN
    )
    allowed = valid[None] & (key_pos >= 0)[:, None, :]
    allowed = allowed[:, None, None]
    head_sink_logit = sink_logit_table.reshape(kv_local, group_count)[None, :, :, None, None]
    masked = jnp.where(allowed, scores, -1e30)
    ceiling = jnp.maximum(jnp.max(masked, axis=-1, keepdims=True), head_sink_logit)
    powers = jnp.where(allowed, jnp.exp(masked - ceiling), 0.0)
    denom = jnp.sum(powers, axis=-1, keepdims=True) + jnp.exp(head_sink_logit - ceiling)
    probs = (powers / denom).astype(jnp.bfloat16)
    output = jnp.einsum("nkgqs,nskd->nqkgd", probs, value_band, preferred_element_type=jnp.float32)
    return output.astype(jnp.bfloat16).reshape(row_count, queries.shape[1])


def rounded(values):
    return lax.optimization_barrier(values.astype(jnp.bfloat16)).astype(jnp.float32)


def body(
    queries,
    key_heads,
    projected_value_heads,
    sink_logit_table,
    out_weight,
    residual,
    norm_gain,
    up_weight,
    down_weight,
):
    row_count = queries.shape[0]
    offset = lax.axis_index("sp") * row_count
    tail = jnp.concatenate(
        [key_heads[row_count - WINDOW_SPAN :], projected_value_heads[row_count - WINDOW_SPAN :]],
        axis=1,
    )
    previous = shifted(tail, "sp", 1)
    attended = attend(queries, key_heads, projected_value_heads, sink_logit_table, previous, offset)
    partial_value = rounded(jnp.dot(attended, out_weight, preferred_element_type=jnp.float32))
    mixed_sum = lax.psum_scatter(
        partial_value.astype(jnp.bfloat16), "tp", scatter_dimension=1, tiled=True
    ).astype(jnp.float32)
    stream = rounded(residual.astype(jnp.float32) + mixed_sum)
    squares = lax.psum(jnp.sum(stream * stream, axis=1, keepdims=True), "tp")
    normed = (stream * lax.rsqrt(squares / D + epsilon) * norm_gain.astype(jnp.float32)).astype(
        jnp.bfloat16
    )
    normed_whole = lax.all_gather(normed, "tp", axis=1, tiled=True)
    hidden_pre = jnp.dot(
        normed_whole,
        lax.all_gather(up_weight, "sp", axis=0, tiled=True),
        preferred_element_type=jnp.float32,
    )
    activated = jnp.square(jax.nn.relu(hidden_pre)).astype(jnp.bfloat16)
    terms = jnp.dot(
        activated,
        lax.all_gather(down_weight, "sp", axis=1, tiled=True),
        preferred_element_type=jnp.float32,
    )
    branch_sum = lax.psum_scatter(
        rounded(terms).astype(jnp.bfloat16), "tp", scatter_dimension=1, tiled=True
    ).astype(jnp.float32)
    return (stream + branch_sum).astype(jnp.bfloat16)


def solution(mesh):
    return jax.shard_map(
        body,
        mesh=mesh,
        in_specs=(
            P("sp", "tp"),
            P("sp", "tp"),
            P("sp", "tp"),
            P("tp"),
            P("tp", None),
            P("sp", "tp"),
            P("tp"),
            P("sp", "tp"),
            P("tp", "sp"),
        ),
        out_specs=P("sp", "tp"),
        check_vma=False,
    )
```

profile of v0, /device:TPU:0, one launch (start us, length us, event | category | flops | bytes accessed | tf_op | source)
XLA Modules:
  0.0 985.8 jit_solution(6724844009850247608)
XLA Ops:
  6.5 0.0 copy-start
  6.5 0.0 copy-start.4
  6.5 0.0 reduce-scatter.3.cloned.1.call-start
  6.5 0.9 slice.32
  7.5 0.8 slice.33
  8.2 4.9 collective-permute-start
  13.2 0.1 add_compare_fusion
  13.3 1.0 broadcast_and_fusion
  14.3 2.0 reshape.91
  16.3 2.0 reshape.89
  18.3 1.4 copy.20
  19.7 1.1 copy.35
  20.8 1.9 copy.19
  22.7 0.7 max.26
  23.4 1.9 copy.15
  25.3 0.0 collective-permute-done
  25.3 0.0 copy-done.4
  25.3 1.7 pad_maximum_fusion
  27.0 1.2 reshape.90
  28.2 1.0 copy.18
  29.1 0.0 copy-start.5
  29.2 2.5 fusion
  31.6 0.0 copy-start.3
  31.7 0.1 broadcast_maximum_fusion
  31.7 2.6 copy-done.3
  34.3 2.8 fusion.1
  37.1 0.1 exponential_add_fusion
  37.2 0.2 reshape.88
  37.5 0.4 copy.14
  37.8 0.0 copy-done.5
  37.9 4.9 fusion.8
  42.7 0.5 copy.23
  43.3 0.0 copy-done
  43.3 0.0 copy-start.6
  43.3 5.4 convolution_convert_fusion.1
  48.7 0.0 reduce-scatter.3.cloned.1.call-update
  48.7 0.0 all-gather.4.cloned.1.call-start
  48.8 0.0 copy-done.6
  48.8 58.3 %reduce-scatter.3.cloned.1.call-done = bf16[1024,768]{1,0:T(8,128)(2,1)} async-done(((bf16[1024,3072]{1,0:T(8,128)(2,1)}), bf16[1024,768]{1,0:T(8,128)(2,1)}) %reduce-scatter.3.cloned.1.call-update) | async-done | bytes 1572880 | tf_op jit(solution)/shard_map/reduce_scatter | solution.py:83
  107.1 2.3 add_convert_fusion
  109.3 0.0 copy-start.2
  109.3 0.4 fusion.2
  109.7 5.8 psum.7
  115.5 1.5 fusion.4
  117.0 0.0 all-gather.4.cloned.1.call-update
  117.1 0.0 all-gather.6.cloned.1.call-start
  117.1 0.7 all-gather.6.cloned.1.call-update
  117.8 0.0 all-gather.8.cloned.1.call-start
  117.9 0.5 all-gather.8.cloned.1.call-update
  118.4 0.2 reduce-scatter.5.cloned.1.call-start
  118.6 45.6 %all-gather.4.cloned.1.call-done = bf16[1024,3072]{1,0:T(8,128)(2,1)} async-done(((bf16[1024,768]{1,0:T(8,128)(2,1)}), bf16[1024,3072]{1,0:T(8,128)(2,1)}) %all-gather.4.cloned.1.call-update) | async-done | bytes 6291472 | tf_op jit(solution)/shard_map/all_gather | solution.py:91
  164.2 364.0 %all-gather.6.cloned.1.call-done = bf16[3072,3072]{1,0:T(8,128)(2,1)} async-done(((bf16[384,3072]{1,0:T(8,128)(2,1)}), bf16[3072,3072]{1,0:T(8,128)(2,1)}) %all-gather.6.cloned.1.call-update) | async-done | bytes 18874384 | tf_op jit(solution)/shard_map/all_gather | solution.py:94
  528.2 25.8 %multiply_convert_fusion.clone.4 = bf16[1024,3072]{1,0:T(8,128)(2,1)} fusion(bf16[1024,3072]{1,0:T(8,128)(2,1)} %all-gather.4.cloned.1.call-done, bf16[3072,3072]{1,0:T(8,128)(2,1)} %all-gather.6.cloned.1.call-done), kind=kOutput, calls=%fused_computation.clone.clone.clone.1 | convolution fusion | flops 19336790016 | bytes 31457280 | tf_op jit(solution)/shard_map/dot_general | solution.py:92
  553.9 0.0 copy-done.2
  553.9 338.0 %all-gather.8.cloned.1.call-done = bf16[3072,3072]{1,0:T(8,128)(2,1)} async-done(((bf16[3072,384]{1,0:T(8,128)(2,1)}), bf16[3072,3072]{1,0:T(8,128)(2,1)}) %all-gather.8.cloned.1.call-update) | async-done | bytes 18874384 | tf_op jit(solution)/shard_map/all_gather | solution.py:100
  892.0 0.0 copy-start.1
  892.0 25.8 %convolution_convert_fusion = bf16[1024,3072]{1,0:T(8,128)(2,1)} fusion(bf16[3072,3072]{1,0:T(8,128)(2,1)} %all-gather.8.cloned.1.call-done, bf16[1024,3072]{1,0:T(8,128)(2,1)} %multiply_convert_fusion.clone.4), kind=kOutput, calls=%fused_computation.4 | convolution fusion | flops 19330498560 | bytes 31457280 | tf_op jit(solution)/shard_map/dot_general | solution.py:98
  917.8 0.0 reduce-scatter.5.cloned.1.call-update
  917.9 58.0 %reduce-scatter.5.cloned.1.call-done = bf16[1024,768]{1,0:T(8,128)(2,1)} async-done(((bf16[1024,3072]{1,0:T(8,128)(2,1)}), bf16[1024,768]{1,0:T(8,128)(2,1)}) %reduce-scatter.5.cloned.1.call-update) | async-done | bytes 1572880 | tf_op jit(solution)/shard_map/reduce_scatter | solution.py:103
  975.9 3.4 fusion.5
  979.3 0.0 copy-done.1
  (7 shorter events, 0.1 us)
Async XLA Ops:
  6.5 36.7 %copy-start = (bf16[384,3072]{1,0:T(8,128)(2,1)S(1)}, bf16[384,3072]{1,0:T(8,128)(2,1)}, u32[]{:S(2)}) copy-start(bf16[384,3072]{1,0:T(8,128)(2,1)} %param.13) | copy-start | bytes 7077892
  6.5 18.8 %copy-start.4 = (bf16[1024,128]{1,0:T(8,128)(2,1)S(1)}, bf16[1024,128]{1,0:T(8,128)(2,1)}, u32[]{:S(2)}) copy-start(bf16[1024,128]{1,0:T(8,128)(2,1)} %param.10) | copy-start | bytes 786436
  6.5 100.5 %reduce-scatter.3.cloned.1.call-start = ((), (), s32[]{:S(2)}) async-start(), calls=%async_computation.2 | async-start | bytes 7864320 | tf_op jit(solution)/shard_map/reduce_scatter | solution.py:83
  8.2 17.1 %collective-permute-start = (bf16[128,256]{1,0:T(8,128)(2,1)S(1)}, bf16[128,256]{1,0:T(8,128)(2,1)S(1)}, u32[]{:S(2)}, u32[]{:S(2)}) collective-permute-start(bf16[128,256]{1,0:T(8,128)(2,1)S(1)} %pad_maximum_fusion.2), channel_id=1, source_target_pairs={{0,4},{4,8},{8,12},{12,16},{16,20},{20,24},{24,28},{1,5},{5,9},{9,... | collective-permute-start | bytes 196616 | tf_op jit(solution)/shard_map/ppermute | solution.py:15
  29.1 8.7 copy-start.5
  31.6 2.7 copy-start.3
  43.3 5.5 copy-start.6
  48.7 115.5 %all-gather.4.cloned.1.call-start = ((), (), s32[]{:S(2)}) async-start(), calls=%async_computation.3 | async-start | bytes 7864320 | tf_op jit(solution)/shard_map/all_gather | solution.py:91
  109.3 444.6 %copy-start.2 = (bf16[1024,768]{1,0:T(8,128)(2,1)}, bf16[1024,768]{1,0:T(8,128)(2,1)S(1)}, u32[]{:S(2)}) copy-start(bf16[1024,768]{1,0:T(8,128)(2,1)S(1)} %add_convert_fusion) | copy-start | bytes 4718596
  117.1 411.1 %all-gather.6.cloned.1.call-start = ((), (), s32[]{:S(2)}) async-start(), calls=%async_computation.4 | async-start | bytes 21233664 | tf_op jit(solution)/shard_map/all_gather | solution.py:94
  117.8 774.2 %all-gather.8.cloned.1.call-start = ((), (), s32[]{:S(2)}) async-start(), calls=%async_computation.5 | async-start | bytes 21233664 | tf_op jit(solution)/shard_map/all_gather | solution.py:100
  118.4 857.5 %reduce-scatter.5.cloned.1.call-start = ((), (), s32[]{:S(2)}) async-start(), calls=%async_computation.6 | async-start | bytes 7864320 | tf_op jit(solution)/shard_map/reduce_scatter | solution.py:103
  892.0 87.3 %copy-start.1 = (bf16[384,3072]{1,0:T(8,128)(2,1)S(1)}, bf16[384,3072]{1,0:T(8,128)(2,1)}, u32[]{:S(2)}) copy-start(bf16[384,3072]{1,0:T(8,128)(2,1)} %param.13) | copy-start | bytes 7077892
Sparse Core Ops, SparseCore 0:
  48.8 58.1 reduce-scatter.2
  117.2 46.9 all-gather.3
  165.8 362.3 all-gather.5
  529.6 362.3 all-gather.7
  918.0 57.8 reduce-scatter.4
where the time goes:
time: 986 us
  waiting for transfers between devices  865 us (88%)
  matrix products  64.4 us (7%)
  local copies, waits for them, and re-layouts  18.5 us (2%)
  other arithmetic  13.4 us (1%)
  between operations  13.3 us (1%)
    all_gather x1, waiting for transfers between devices, body(): lax.all_gather(up_weight, 'sp', axis=0, tiled=True)  364 us
    all_gather x1, waiting for transfers between devices, body(): lax.all_gather(down_weight, 'sp', axis=1, tiled=True)  338 us
    reduce_scatter x1, waiting for transfers between devices, body(): lax.psum_scatter(partial_value.astype(jnp.bfloat16), 'tp', scatter_dimens...  58.3 us
    reduce_scatter x1, waiting for transfers between devices, body(): lax.psum_scatter(rounded(terms).astype(jnp.bfloat16), 'tp', scatter_dimen...  58 us
    all_gather x1, waiting for transfers between devices, body(): normed_whole = lax.all_gather(normed, 'tp', axis=1, tiled=True)  45.6 us
    dot_general x1, matrix products, body(): jnp.dot(activated, lax.all_gather(down_weight, 'sp', axis=1, tiled=True),...  25.8 us
    dot_general x1, matrix products, body(): jnp.dot(normed_whole, lax.all_gather(up_weight, 'sp', axis=0, tiled=True)...  25.8 us
  transfers between devices with their start and end apart: 6, of which 5 were waited for; matrix products, arithmetic and copies ran while one was open for 4% of the time, Pallas kernels for 0%

commit v1 on v0

--- a/solution.py
+++ b/solution.py
@@ -97,7 +97,7 @@
     activated = jnp.square(jax.nn.relu(hidden_pre)).astype(jnp.bfloat16)
     terms = jnp.dot(
         activated,
-        lax.all_gather(down_weight, "sp", axis=1, tiled=True),
+        jnp.concatenate(lax.all_gather(down_weight, "sp"), axis=1),
         preferred_element_type=jnp.float32,
     )
     branch_sum = lax.psum_scatter(

time: 986 us -> 946 us (0.959)
  waiting for transfers between devices: 865 us -> 799 us
  local copies, waits for them, and re-layouts: 18.5 us -> 43.3 us
    all_gather x1, waiting for transfers between devices: 338 us -> 295 us  [body(): lax.all_gather(down_weight, 'sp')]
    reshape x0 -> x1, local copies, waits for them, and re-layouts: none -> 24.8 us  [body(): jnp.concatenate(lax.all_gather(down_weight, 'sp'), axis=1)]
    all_gather x1, waiting for transfers between devices: 45.6 us -> 22.9 us  [body(): normed_whole = lax.all_gather(normed, 'tp', axis=1, tiled=True)]
where the time goes in v1:
time: 946 us; the launch traced here: 945 us
  waiting for transfers between devices  799 us (84%)
  matrix products  63 us (7%)
  local copies, waits for them, and re-layouts  43.3 us (5%)
  between operations  15.2 us (2%)
  other arithmetic  13.5 us (1%)
    all_gather x1, waiting for transfers between devices, body(): lax.all_gather(up_weight, 'sp', axis=0, tiled=True)  364 us
    all_gather x1, waiting for transfers between devices, body(): lax.all_gather(down_weight, 'sp')  295 us
    reduce_scatter x1, waiting for transfers between devices, body(): lax.psum_scatter(rounded(terms).astype(jnp.bfloat16), 'tp', scatter_dimen...  58 us
    reduce_scatter x1, waiting for transfers between devices, body(): lax.psum_scatter(partial_value.astype(jnp.bfloat16), 'tp', scatter_dimens...  57.7 us
    dot_general x1, matrix products, body(): jnp.dot(normed_whole, lax.all_gather(up_weight, 'sp', axis=0, tiled=True)...  25.7 us
    reshape x1, local copies, waits for them, and re-layouts, body(): jnp.concatenate(lax.all_gather(down_weight, 'sp'), axis=1)  24.8 us
    dot_general x1, matrix products, body(): jnp.dot(activated, jnp.concatenate(lax.all_gather(down_weight, 'sp'), axi...  24.5 us
    all_gather x1, waiting for transfers between devices, body(): normed_whole = lax.all_gather(normed, 'tp', axis=1, tiled=True)  22.9 us
  transfers between devices with their start and end apart: 6, of which 5 were waited for; matrix products, arithmetic and copies ran while one was open for 4% of the time, Pallas kernels for 0%

profile of v1, /device:TPU:0, one launch (start us, length us, event | category | flops | bytes accessed | tf_op | source)
XLA Modules:
  0.0 944.9 jit_solution(15052837907160689385)
XLA Ops:
  7.4 0.0 copy-start
  7.4 0.0 copy-start.5
  7.4 0.0 reduce-scatter.3.cloned.1.call-start
  7.4 0.9 slice.32
  8.3 0.8 slice.33
  9.1 4.9 collective-permute-start
  14.0 0.1 add_compare_fusion
  14.1 1.0 broadcast_and_fusion
  15.1 2.0 reshape.100
  17.1 2.0 reshape.98
  19.1 1.4 copy.32
  20.5 1.1 copy.48
  21.6 1.9 copy.31
  23.5 0.7 max.26
  24.2 1.9 copy.27
  26.1 0.0 collective-permute-done
  26.1 0.0 copy-done.5
  26.1 1.7 pad_maximum_fusion
  27.8 1.2 reshape.99
  29.0 1.0 copy.30
  29.9 0.0 copy-start.6
  29.9 2.5 fusion
  32.4 0.0 copy-start.4
  32.5 0.1 broadcast_maximum_fusion
  32.5 2.6 copy-done.4
  35.1 2.8 fusion.1
  37.9 0.1 exponential_add_fusion
  38.0 0.2 reshape.97
  38.3 0.4 copy.26
  38.6 0.0 copy-done.6
  38.6 4.9 fusion.8
  43.5 0.5 copy.35
  44.0 0.0 copy-done
  44.1 5.4 convolution_convert_fusion.1
  49.4 0.0 copy-start.7
  49.4 0.0 reduce-scatter.3.cloned.1.call-update
  49.5 0.0 all-gather.9.cloned.1.call-start
  49.5 0.5 all-gather.9.cloned.1.call-update
  50.0 0.0 all-gather.5.cloned.1.call-start
  50.1 0.0 copy-done.7
  50.1 57.7 %reduce-scatter.3.cloned.1.call-done = bf16[1024,768]{1,0:T(8,128)(2,1)} async-done(((bf16[1024,3072]{1,0:T(8,128)(2,1)}), bf16[1024,768]{1,0:T(8,128)(2,1)}) %reduce-scatter.3.cloned.1.call-update) | async-done | bytes 1572880 | tf_op jit(solution)/shard_map/reduce_scatter | solution.py:83
  107.8 2.3 add_convert_fusion
  110.1 0.0 copy-start.2
  110.1 0.4 fusion.2
  110.5 6.1 psum.7
  116.6 1.6 fusion.4
  118.2 0.0 all-gather.5.cloned.1.call-update
  118.2 0.0 all-gather.7.cloned.1.call-start
  118.2 0.5 all-gather.7.cloned.1.call-update
  118.8 0.2 reduce-scatter.5.cloned.1.call-start
  119.0 295.2 %all-gather.9.cloned.1.call-done = bf16[24576,384]{1,0:T(8,128)(2,1)} async-done(((bf16[3072,384]{1,0:T(8,128)(2,1)}), bf16[24576,384]{1,0:T(8,128)(2,1)}) %all-gather.9.cloned.1.call-update) | async-done | bytes 18874384 | tf_op jit(solution)/shard_map/all_gather | solution.py:100
  414.2 24.8 %copy.36 = bf16[3072,8,384]{0,2,1:T(8,128)(2,1)} copy(bf16[3072,8,384]{2,0,1:T(8,128)(2,1)} %bitcast.59) | data formatting | bytes 37748736 | tf_op jit(solution)/shard_map/reshape | solution.py:100
  439.0 0.0 copy-done.2
  439.0 22.9 %all-gather.5.cloned.1.call-done = bf16[1024,3072]{1,0:T(8,128)(2,1)} async-done(((bf16[1024,768]{1,0:T(8,128)(2,1)}), bf16[1024,3072]{1,0:T(8,128)(2,1)}) %all-gather.5.cloned.1.call-update) | async-done | bytes 6291472 | tf_op jit(solution)/shard_map/all_gather | solution.py:91
  461.9 363.8 %all-gather.7.cloned.1.call-done = bf16[3072,3072]{1,0:T(8,128)(2,1)} async-done(((bf16[384,3072]{1,0:T(8,128)(2,1)}), bf16[3072,3072]{1,0:T(8,128)(2,1)}) %all-gather.7.cloned.1.call-update) | async-done | bytes 18874384 | tf_op jit(solution)/shard_map/all_gather | solution.py:94
  825.7 0.0 copy-start.3
  825.7 25.7 %multiply_convert_fusion.clone.4 = bf16[1024,3072]{1,0:T(8,128)(2,1)} fusion(bf16[1024,3072]{1,0:T(8,128)(2,1)} %all-gather.5.cloned.1.call-done, bf16[3072,3072]{1,0:T(8,128)(2,1)} %all-gather.7.cloned.1.call-done), kind=kOutput, calls=%fused_computation.clone.clone.clone.1 | convolution fusion | flops 19336790016 | bytes 31457280 | tf_op jit(solution)/shard_map/dot_general | solution.py:92
  851.4 0.0 copy-done.3
  851.4 0.0 copy-start.1
  851.4 24.5 %convolution_convert_fusion = bf16[1024,3072]{1,0:T(8,128)(2,1)} fusion(bf16[3072,3072]{0,1:T(8,128)(2,1)S(1)} %bitcast.60, bf16[1024,3072]{1,0:T(8,128)(2,1)} %multiply_convert_fusion.clone.4), kind=kOutput, calls=%fused_computation.4 | convolution fusion | flops 19330498560 | bytes 31457280 | tf_op jit(solution)/shard_map/dot_general | solution.py:98
  875.9 0.0 reduce-scatter.5.cloned.1.call-update
  876.0 58.0 %reduce-scatter.5.cloned.1.call-done = bf16[1024,768]{1,0:T(8,128)(2,1)} async-done(((bf16[1024,3072]{1,0:T(8,128)(2,1)}), bf16[1024,768]{1,0:T(8,128)(2,1)}) %reduce-scatter.5.cloned.1.call-update) | async-done | bytes 1572880 | tf_op jit(solution)/shard_map/reduce_scatter | solution.py:103
  933.9 3.4 fusion.5
  937.4 0.0 copy-done.1
  (7 shorter events, 0.1 us)
Async XLA Ops:
  7.4 36.7 %copy-start = (bf16[384,3072]{1,0:T(8,128)(2,1)S(1)}, bf16[384,3072]{1,0:T(8,128)(2,1)}, u32[]{:S(2)}) copy-start(bf16[384,3072]{1,0:T(8,128)(2,1)} %param.13) | copy-start | bytes 7077892
  7.4 18.7 %copy-start.5 = (bf16[1024,128]{1,0:T(8,128)(2,1)S(1)}, bf16[1024,128]{1,0:T(8,128)(2,1)}, u32[]{:S(2)}) copy-start(bf16[1024,128]{1,0:T(8,128)(2,1)} %param.10) | copy-start | bytes 786436
  7.4 100.4 %reduce-scatter.3.cloned.1.call-start = ((), (), s32[]{:S(2)}) async-start(), calls=%async_computation.2 | async-start | bytes 7864320 | tf_op jit(solution)/shard_map/reduce_scatter | solution.py:83
  9.1 17.0 %collective-permute-start = (bf16[128,256]{1,0:T(8,128)(2,1)S(1)}, bf16[128,256]{1,0:T(8,128)(2,1)S(1)}, u32[]{:S(2)}, u32[]{:S(2)}) collective-permute-start(bf16[128,256]{1,0:T(8,128)(2,1)S(1)} %pad_maximum_fusion.2), channel_id=1, source_target_pairs={{0,4},{4,8},{8,12},{12,16},{16,20},{20,24},{24,28},{1,5},{5,9},{9,... | collective-permute-start | bytes 196616 | tf_op jit(solution)/shard_map/ppermute | solution.py:15
  29.9 8.7 copy-start.6
  32.4 2.7 copy-start.4
  49.4 0.7 copy-start.7
  49.5 364.7 %all-gather.9.cloned.1.call-start = ((), (), s32[]{:S(2)}) async-start(), calls=%async_computation.6 | async-start | bytes 21233664 | tf_op jit(solution)/shard_map/all_gather | solution.py:100
  50.0 411.8 %all-gather.5.cloned.1.call-start = ((), (), s32[]{:S(2)}) async-start(), calls=%async_computation.3 | async-start | bytes 7864320 | tf_op jit(solution)/shard_map/all_gather | solution.py:91
  110.1 328.9 %copy-start.2 = (bf16[1024,768]{1,0:T(8,128)(2,1)}, bf16[1024,768]{1,0:T(8,128)(2,1)S(1)}, u32[]{:S(2)}) copy-start(bf16[1024,768]{1,0:T(8,128)(2,1)S(1)} %add_convert_fusion) | copy-start | bytes 4718596
  118.2 707.5 %all-gather.7.cloned.1.call-start = ((), (), s32[]{:S(2)}) async-start(), calls=%async_computation.4 | async-start | bytes 21233664 | tf_op jit(solution)/shard_map/all_gather | solution.py:94
  118.8 815.2 %reduce-scatter.5.cloned.1.call-start = ((), (), s32[]{:S(2)}) async-start(), calls=%async_computation.5 | async-start | bytes 7864320 | tf_op jit(solution)/shard_map/reduce_scatter | solution.py:103
  825.7 25.7 %copy-start.3 = (bf16[3072,8,384]{0,2,1:T(8,128)(2,1)S(1)}, bf16[3072,8,384]{0,2,1:T(8,128)(2,1)}, u32[]{:S(2)}) copy-start(bf16[3072,8,384]{0,2,1:T(8,128)(2,1)} %copy.36) | copy-start | bytes 56623108
  851.4 86.0 %copy-start.1 = (bf16[384,3072]{1,0:T(8,128)(2,1)S(1)}, bf16[384,3072]{1,0:T(8,128)(2,1)}, u32[]{:S(2)}) copy-start(bf16[384,3072]{1,0:T(8,128)(2,1)} %param.13) | copy-start | bytes 7077892
Sparse Core Ops, SparseCore 0:
  49.6 58.1 reduce-scatter.2
  876.1 57.8 reduce-scatter.4
Sparse Core Ops, SparseCore 1:
  51.5 362.7 all-gather.8
  415.6 46.2 all-gather.4
  463.3 362.3 all-gather.6
